TPU v7x, 32 devices: a whole 2x2x4 slice. The times are simulated.
32 devices in a mesh: grp: 2 (over y), sp: 4 (over z), tp: 4 (over x, core).
Axes of the slice: x: 2, y: 2, z: 4, core: 2. Of those that a mesh axis runs over, the one named last changes fastest.
Arguments:
- tokens: bfloat16 [4096, 2048], P(('grp', 'sp')), parts along dimension 0, may hold values from -6 to 6
- fresh_token_input: bfloat16 [4096], P('grp'), parts along dimension 0, may hold values from -6 to 6
- value_matrix: bfloat16 [2048, 2048], P(None, 'tp'), may hold values from -0.125 to 0.125
- write_matrix: bfloat16 [2048, 1024], P(None, 'tp'), may hold values from -0.125 to 0.125
- read_matrix: bfloat16 [2048, 1024], P(None, 'tp'), may hold values from -0.125 to 0.125
- gate_matrix: bfloat16 [2048, 2048], P(None, 'tp'), may hold values from -0.125 to 0.125
- step_matrix: bfloat16 [2048, 32], replicated, may hold values from -0.125 to 0.125
- value_filter_taps: bfloat16 [4, 2048], replicated, may hold values from -3 to 3
- write_filter_taps: bfloat16 [4, 1024], replicated, may hold values from -3 to 3
- read_filter_taps: bfloat16 [4, 1024], replicated, may hold values from -3 to 3
- head_log_decay: float32 [32], replicated
- step_offset_bias: float32 [32], replicated, may hold values from -3.5 to -2.5
- decay_spike: float32 [4096, 32], P(('grp', 'sp'), 'tp'), parts along dimension 0, may hold values from -3 to 0, as said below
- bypass_scale: float32 [32], replicated, may hold values from 0.5 to 2
- group_norm_scale: float32 [2048], replicated, may hold values from 0.1 to 1.9
Outputs:
- prompt_out: bfloat16 [4096, 2048], P(('grp', 'sp'), 'tp'), parts along dimension 0
- state_cache: bfloat16 [256, 2048], P(('grp', 'sp'), 'tp'), parts along dimension 0
- step_out: bfloat16 [1024, 4], P(('grp', 'tp'), 'sp'), parts along dimension 0
There are 2 independent parts, one for each index of `grp`. A program takes and returns all parts, laid end to end along the dimension named above; an argument that names none is the same for every part. Nothing has to cross between parts.
Inputs may be any that keep to these rules, and one draw needn't show every extreme that they name: `decay_spike`: never positive.
All inputs are finite; a program needn't handle non-finite values.
Results may differ from a plain program's by a relative error of at most 0.023.
Values may be sent and summed in bfloat16 or wider, within the bound.
A program may use at most 64 MiB of HBM per device.

v0:
```python
import jax
import jax.numpy as jnp
from jax import lax
from jax.sharding import PartitionSpec as P

HEAD = 64
STATE = 128
CONV = 4
BLOCK = 128
epsilon = 1e-06


def passed_along(block, axis, distance):
    devices = range(lax.axis_size(axis))
    route = [(i - distance, i) for i in devices if i - distance in devices]
    return lax.ppermute(block, axis, route)


def from_root(value, axis, source):
    kept = jnp.where(lax.axis_index(axis) == source, value, 0).astype(value.dtype)
    return lax.psum(kept, axis)


def project(operand, weights):
    return jnp.dot(operand, weights, preferred_element_type=jnp.float32).astype(jnp.bfloat16)


def apply_taps(previous, current, tap_weights):
    joined = jnp.concatenate([previous, current], axis=0).astype(jnp.float32)
    length = current.shape[0]
    summed = jnp.zeros(current.shape, jnp.float32)
    for offset in range(CONV):
        summed = summed + tap_weights[offset].astype(jnp.float32) * joined[offset : offset + length]
    return summed


def group_norm(gated_rows, groups):
    shaped = gated_rows.reshape(gated_rows.shape[:-1] + (groups, -1))
    normed = shaped * lax.rsqrt(jnp.mean(shaped * shaped, axis=-1, keepdims=True) + epsilon)
    return normed.reshape(gated_rows.shape)


def read_new(cached, stored_portion, read_part, new_decay, step_now, value_now):
    states = cached.astype(jnp.float32).reshape((cached.shape[0],) + value_now.shape)
    updated = (
        new_decay[None, :, :, None] * states
        + step_now[None, :, :, None] * stored_portion.T[:, :, None, None] * value_now[None]
    )
    return jnp.einsum("gn,ngep->gep", read_part, updated, precision=lax.Precision.HIGHEST)


def on_device(
    tokens,
    fresh_token_input,
    value_matrix,
    write_matrix,
    read_matrix,
    gate_matrix,
    step_matrix,
    value_filter_taps,
    write_filter_taps,
    read_filter_taps,
    head_log_decay,
    step_offset_bias,
    decay_spike,
    bypass_scale,
    group_norm_scale,
):
    head_rank = lax.axis_index("tp")
    sequence_rank = lax.axis_index("sp")
    sequence_count = lax.axis_size("sp")
    channels = value_matrix.shape[1]
    head_count = channels // HEAD
    map_width = write_matrix.shape[1]
    group_count = map_width // STATE
    per_group = head_count // group_count
    row_count = tokens.shape[0]
    head_start = head_rank * head_count
    local_count = STATE // sequence_count
    own_step = lax.dynamic_slice_in_dim(step_matrix, head_start, head_count, 1)
    own_value_taps = lax.dynamic_slice_in_dim(value_filter_taps, head_rank * channels, channels, 1)
    own_write_taps = lax.dynamic_slice_in_dim(
        write_filter_taps, head_rank * map_width, map_width, 1
    )
    own_read_taps = lax.dynamic_slice_in_dim(read_filter_taps, head_rank * map_width, map_width, 1)
    head_decay_rates = jnp.exp(lax.dynamic_slice_in_dim(head_log_decay, head_start, head_count, 0))
    own_bias = lax.dynamic_slice_in_dim(step_offset_bias, head_start, head_count, 0)
    own_skip = lax.dynamic_slice_in_dim(bypass_scale, head_start, head_count, 0)
    own_gain = lax.dynamic_slice_in_dim(group_norm_scale, head_rank * channels, channels, 0)
    value_rows = project(tokens, value_matrix)
    write_rows = project(tokens, write_matrix)
    read_rows = project(tokens, read_matrix)
    gate_rows = project(tokens, gate_matrix)
    step_raw = jnp.dot(tokens, own_step, preferred_element_type=jnp.float32)
    edge = row_count - (CONV - 1)
    tail_rows = (value_rows[edge:], write_rows[edge:], read_rows[edge:])
    before = passed_along((tail_rows[0], tail_rows[1], tail_rows[2]), "sp", 1)
    ending = (
        from_root(tail_rows[0], "sp", sequence_count - 1),
        from_root(tail_rows[1], "sp", sequence_count - 1),
        from_root(tail_rows[2], "sp", sequence_count - 1),
    )
    values = jax.nn.silu(apply_taps(before[0], value_rows, own_value_taps)).astype(jnp.bfloat16)
    writes = jax.nn.silu(apply_taps(before[1], write_rows, own_write_taps)).astype(jnp.bfloat16)
    reads = jax.nn.silu(apply_taps(before[2], read_rows, own_read_taps)).astype(jnp.bfloat16)
    step_length = jax.nn.softplus(step_raw + own_bias)
    log_decay_value = decay_spike - step_length * head_decay_rates
    blocks = row_count // BLOCK
    block_values = values.reshape(blocks, BLOCK, group_count, per_group, HEAD)
    block_writes = writes.reshape(blocks, BLOCK, group_count, STATE)
    block_reads = reads.reshape(blocks, BLOCK, group_count, STATE)
    block_steps = step_length.reshape(blocks, BLOCK, group_count, per_group)
    cumulative = jnp.cumsum(log_decay_value.reshape(blocks, BLOCK, group_count, per_group), axis=1)
    block_end = cumulative[:, -1]
    scaled = (
        (jnp.exp(block_end[:, None] - cumulative) * block_steps)[..., None]
        * block_values.astype(jnp.float32)
    ).astype(jnp.bfloat16)
    block_states = jnp.einsum(
        "bsgn,bsgep->bngep", block_writes, scaled, preferred_element_type=jnp.float32
    )
    running = jnp.zeros((STATE, group_count, per_group, HEAD), jnp.float32)
    inside = []
    for block_index in range(blocks):
        inside.append(running)
        running = (
            jnp.exp(block_end[block_index])[None, :, :, None] * running + block_states[block_index]
        )
    local_states = jnp.stack(inside)
    shard_fading_factor = jnp.sum(block_end, axis=0)
    before_block = jnp.cumsum(block_end, axis=0) - block_end
    decay_table = lax.all_gather(shard_fading_factor[None], "sp", axis=0, tiled=True)
    inclusive = jnp.cumsum(decay_table, axis=0)
    exclusive = inclusive - decay_table
    total_decay = inclusive[-1]
    row_pieces = lax.all_to_all(running[None], "sp", split_axis=1, concat_axis=0, tiled=True)
    ranks = jnp.arange(sequence_count)
    below = (ranks[None, :] < ranks[:, None])[:, :, None, None]
    prefix_weight = jnp.exp(jnp.where(below, exclusive[:, None] - inclusive[None, :], -jnp.inf))
    prefix_rows = jnp.einsum(
        "jkge,kngep->jngep", prefix_weight, row_pieces, precision=lax.Precision.HIGHEST
    )
    final_weight = jnp.exp(total_decay[None] - inclusive)
    final_rows = jnp.einsum(
        "kge,kngep->ngep", final_weight, row_pieces, precision=lax.Precision.HIGHEST
    )
    earlier_state = lax.all_to_all(prefix_rows, "sp", split_axis=0, concat_axis=1, tiled=True)[0]
    scores = jnp.einsum(
        "blgn,bsgn->bgls", block_reads, block_writes, preferred_element_type=jnp.float32
    )
    cum_heads = jnp.transpose(cumulative, (0, 2, 3, 1))
    decay_gaps = cum_heads[..., :, None] - cum_heads[..., None, :]
    step_heads = jnp.transpose(block_steps, (0, 2, 3, 1))
    causal = jnp.tril(jnp.ones((BLOCK, BLOCK), bool))
    mixing = (
        scores[:, :, None]
        * jnp.exp(jnp.where(causal, decay_gaps, -jnp.inf))
        * step_heads[..., None, :]
    ).astype(jnp.bfloat16)
    inner_part = jnp.einsum(
        "bgels,bsgep->blgep", mixing, block_values, preferred_element_type=jnp.float32
    )
    entering = jnp.exp(before_block)[:, None, :, :, None] * earlier_state[None] + local_states
    carried_part = jnp.exp(cumulative)[..., None] * jnp.einsum(
        "blgn,bngep->blgep",
        block_reads.astype(jnp.float32),
        entering,
        precision=lax.Precision.HIGHEST,
    )
    mixed_rows = (inner_part + carried_part).reshape(row_count, head_count, HEAD) + own_skip[
        None, :, None
    ] * values.astype(jnp.float32).reshape(row_count, head_count, HEAD)
    gated_rows = mixed_rows.reshape(row_count, channels) * jax.nn.silu(
        gate_rows.astype(jnp.float32)
    )
    prompt_out = (group_norm(gated_rows, group_count) * own_gain).astype(jnp.bfloat16)
    new_row = fresh_token_input[None]
    new_value = project(new_row, value_matrix)
    new_write = project(new_row, write_matrix)
    new_read = project(new_row, read_matrix)
    new_gate = project(new_row, gate_matrix)
    new_step = jax.nn.softplus(
        jnp.dot(new_row, own_step, preferred_element_type=jnp.float32)[0] + own_bias
    )
    new_values = jax.nn.silu(apply_taps(ending[0], new_value, own_value_taps)).astype(jnp.bfloat16)
    latest_stores = jax.nn.silu(apply_taps(ending[1], new_write, own_write_taps)).astype(
        jnp.bfloat16
    )
    new_reads = jax.nn.silu(apply_taps(ending[2], new_read, own_read_taps)).astype(jnp.bfloat16)
    value_now = new_values.astype(jnp.float32).reshape(group_count, per_group, HEAD)
    write_now = latest_stores.astype(jnp.float32).reshape(group_count, STATE)
    read_now = new_reads.astype(jnp.float32).reshape(group_count, STATE)
    new_decay = jnp.exp(-new_step * head_decay_rates).reshape(group_count, per_group)
    step_now = new_step.reshape(group_count, per_group)
    row_start = sequence_rank * local_count
    cache_rows = final_rows.reshape(local_count, channels).astype(jnp.bfloat16)
    stored_portion = lax.dynamic_slice_in_dim(write_now, row_start, local_count, 1)
    read_part = lax.dynamic_slice_in_dim(read_now, row_start, local_count, 1)
    partial_value = read_new(cache_rows, stored_portion, read_part, new_decay, step_now, value_now)
    reading = lax.psum(partial_value, "sp")
    new_mixed = reading + own_skip.reshape(group_count, per_group)[:, :, None] * value_now
    new_gated = new_mixed.reshape(1, channels) * jax.nn.silu(new_gate.astype(jnp.float32))
    step_whole = (group_norm(new_gated, group_count) * own_gain).astype(jnp.bfloat16)[0]
    step_table = step_whole.reshape(channels // sequence_count, sequence_count)
    step_out = lax.dynamic_slice_in_dim(step_table, sequence_rank, 1, 1)
    return (prompt_out, cache_rows, step_out)


def solution(mesh):
    placed = (
        P(("grp", "sp"), None),
        P("grp"),
        P(None, "tp"),
        P(None, "tp"),
        P(None, "tp"),
        P(None, "tp"),
        P(),
        P(),
        P(),
        P(),
        P(),
        P(),
        P(("grp", "sp"), "tp"),
        P(),
        P(),
    )
    return jax.shard_map(
        on_device,
        mesh=mesh,
        in_specs=placed,
        out_specs=(P(("grp", "sp"), "tp"), P(("grp", "sp"), "tp"), P(("grp", "tp"), "sp")),
        check_vma=False,
    )
```

profile of v0, /device:TPU:0, one launch (start us, length us, event | category | flops | bytes accessed | tf_op | source)
XLA Modules:
  0.0 126.4 jit_solution(4960432107386798171)
XLA Ops:
  0.7 1.6 %copy-done = bf16[512,2048]{1,0:T(8,128)(2,1)S(1)} copy-done((bf16[512,2048]{1,0:T(8,128)(2,1)S(1)}, bf16[512,2048]{1,0:T(8,128)(2,1)}, u32[]{:S(2)}) %copy-start) | copy-done | bytes 2097176
  2.2 1.9 %convolution_convert_fusion.2 = bf16[512,256]{1,0:T(8,128)(2,1)S(1)} fusion(bf16[512,2048]{1,0:T(8,128)(2,1)S(1)} %copy-done, bf16[2048,256]{1,0:T(8,128)(2,1)} %param.18), kind=kOutput, calls=%fused_computation.11 | convolution fusion | flops 537001984 | bytes 3407872 | tf_op jit(solution)/shard_map/dot_general | solution.py:25
  4.7 5.7 %collective-permute-start.2 = (bf16[3,256]{1,0:T(4,128)(2,1)}, bf16[3,256]{1,0:T(4,128)(2,1)}, u32[]{:S(2)}, u32[]{:S(2)}) collective-permute-start(bf16[3,256]{1,0:T(4,128)(2,1)} %get-tuple-element.57), channel_id=1, source_target_pairs={{0,4},{4,8},{8,12},{1,5},{5,9},{9,13},{2,6},{6,10},{10,14},{3,7},{... | collective-permute-start | bytes 4616 | tf_op jit(solution)/shard_map/ppermute | solution.py:16
  10.4 0.7 convolution_convert_fusion.3
  11.8 3.6 %collective-permute-start.1 = (bf16[3,256]{1,0:T(4,128)(2,1)}, bf16[3,256]{1,0:T(4,128)(2,1)}, u32[]{:S(2)}, u32[]{:S(2)}) collective-permute-start(bf16[3,256]{1,0:T(4,128)(2,1)} %get-tuple-element.54), channel_id=1, source_target_pairs={{0,4},{4,8},{8,12},{1,5},{5,9},{9,13},{2,6},{6,10},{10,14},{3,7},{... | collective-permute-start | bytes 4616 | tf_op jit(solution)/shard_map/ppermute | solution.py:16
  15.4 1.3 convolution_convert_fusion.1
  16.7 0.8 copy-done.8
  18.1 3.5 %collective-permute-start = (bf16[3,512]{1,0:T(4,128)(2,1)}, bf16[3,512]{1,0:T(4,128)(2,1)}, u32[]{:S(2)}, u32[]{:S(2)}) collective-permute-start(bf16[3,512]{1,0:T(4,128)(2,1)} %get-tuple-element.52), channel_id=1, source_target_pairs={{0,4},{4,8},{8,12},{1,5},{5,9},{9,13},{2,6},{6,10},{10,14},{3,7},{... | collective-permute-start | bytes 9224 | tf_op jit(solution)/shard_map/ppermute | solution.py:16
  22.4 1.5 %fusion.96 = f32[1,256]{1,0:T(1,128)S(1)} fusion(bf16[2048,1]{0,1:T(2,128)(2,1)S(1)} %reshape.251, bf16[2048,256]{1,0:T(8,128)(2,1)} %param.19), kind=kOutput, calls=%fused_computation.194 | convolution fusion | flops 1048576 | bytes 1053696 | tf_op jit(solution)/shard_map/dot_general | solution.py:25
  27.1 2.0 %fusion.99 = f32[1,512]{1,0:T(1,128)S(1)} fusion(bf16[2048,1]{0,1:T(2,128)(2,1)S(1)} %reshape.251, bf16[2048,512]{1,0:T(8,128)(2,1)} %param.20), kind=kOutput, calls=%fused_computation.197 | convolution fusion | flops 2097152 | bytes 2103296 | tf_op jit(solution)/shard_map/dot_general | solution.py:25
  29.1 7.6 %all-gather.1 = f32[4,2,4]{2,1,0:T(2,128)S(1)} all-gather(f32[1,2,4]{2,1,0:T(2,128)S(1)} %bitcast.152), channel_id=2, replica_groups=mesh['grp'=2,'sp'=4,'tp'=4] {'sp'}, dimensions={0}, use_global_device_ids=true | all-gather | bytes 160 | tf_op jit(solution)/shard_map/all_gather | solution.py:132
  36.7 10.5 %all-reduce = (bf16[3,512]{1,0:T(4,128)(2,1)S(1)}, bf16[3,256]{1,0:T(4,128)(2,1)S(1)}, bf16[3,256]{1,0:T(4,128)(2,1)S(1)}) all-reduce(bf16[3,512]{1,0:T(4,128)(2,1)S(1)} %get-tuple-element.53, bf16[3,256]{1,0:T(4,128)(2,1)S(1)} %get-tuple-element.56, ...), channel_id=1, replica_groups=mesh['grp'=2,'sp'=4,'tp'=4] {'sp'}, use_global_device_ids=true, to_apply=%region_7.8 | all-reduce | flops 3072 | bytes 12288 | tf_op jit(solution)/shard_map/psum | solution.py:21
  48.1 1.0 copy.149
  49.2 0.7 convert_reduce_fusion.1
  49.9 2.4 %fusion.90 = (f32[4,128,2,4]{3,2,1,0:T(2,128)}, f32[4,128,2,4]{3,2,1,0:T(2,128)S(1)}) fusion(f32[4,128,2,4]{3,2,1,0:T(2,128)S(1)} %fusion.94, f32[4,128,2,4]{3,2,1,0:T(2,128)} %copy.149, f32[4,2,4]{2,1,0:T(2,128)S(1)} %get-tuple-element.47), kind=kLoop, calls=%fused_computation.187 | loop fusion | flops 8192 | bytes 65664 | tf_op jit(solution)/shard_map/exp | solution.py:164
  52.4 0.7 convert_reduce_fusion
  53.7 0.7 dynamic_slice.39
  55.9 1.3 %mul.529 = f32[2,4]{1,0:T(2,128)} reshape(f32[8]{0:T(128)} %get-tuple-element.28) | data formatting | bytes 64 | tf_op jit(solution)/shard_map/mul | solution.py:46
  57.6 1.3 %copy.148 = f32[4,128,2,4]{1,3,2,0:T(4,128)S(1)} copy(f32[4,128,2,4]{3,2,1,0:T(2,128)} %get-tuple-element.44) | data formatting | bytes 32768 | tf_op jit(solution)/shard_map/exp | solution.py:164
  59.7 0.7 maximum_convert_fusion.2
  60.5 1.0 multiply_convert_fusion.5
  61.5 0.8 maximum_convert_fusion.1
  62.8 0.8 maximum_convert_fusion
  63.6 1.3 %multiply_convert_fusion.4 = bf16[512,512]{1,0:T(8,128)(2,1)S(1)} fusion(f32[515,512]{1,0:T(8,128)S(1)} %maximum_convert_fusion, f32[512]{0:T(512)} %bitcast.141, f32[512]{0:T(512)} %bitcast.140, f32[512]{0:T(512)S(1)} %bitcast.139, f32[512]{0:T(512)S(1)} %bitcast.138), kind=kLoop, calls=%fused_computation.44 | loop fusion | flops 3145728 | bytes 4726784 | tf_op jit(solution)/shard_map/convert_element_type | solution.py:103
  65.0 1.0 copy.140
  66.0 2.0 %reshape.229 = bf16[4,128,2,4,64]{1,0,4,3,2:T(4,128)(2,1)} reshape(bf16[512,512]{0,1:T(8,128)(2,1)} %copy.140) | data formatting | bytes 1048576 | tf_op jit(solution)/shard_map/reshape | solution.py:109
  68.0 1.3 multiply_convert_fusion.3
  69.5 1.0 slice_add_fusion
  70.8 1.2 reshape.274
  72.0 3.6 %all-to-all-start = ((f32[4,1,16384]{2,1,0:T(1,128)}), f32[4,1,16384]{2,1,0:T(1,128)S(1)}, u32[]{:S(2)}, u32[]{:S(2)}) async-start(f32[4,1,16384]{2,1,0:T(1,128)} %reshape.274), calls=%async_computation | async-start | bytes 524288 | tf_op jit(solution)/shard_map/all_to_all | solution.py:136
  75.9 3.0 %convolution_bitcast_fusion.2 = f32[4,128,2,4,64]{1,4,3,2,0:T(8,128)} fusion(f32[4,2,4,128]{3,2,1,0:T(4,128)S(1)} %copy.146, f32[4,2,4,128]{3,2,1,0:T(4,128)S(1)} %copy.144, f32[4,2,128,128]{3,2,1,0:T(8,128)S(1)} %fusion.40, pred[128,128]{1,0:T(8,128)(4,1)S(1)} %iota_compare_fusion, bf16[4,128,2,4,64]{1,0,4,3,2:T(4,128)(2,1)} %reshape.229), kind=kOutput, calls=%fused_computation.5 | convolution fusion | flops 69730304 | bytes 2146304 | tf_op jit(solution)/shard_map/bgels,bsgep->blgep/dot_general | solution.py:160
  78.8 3.3 %all-to-all-done = f32[4,1,16384]{2,1,0:T(1,128)S(1)} async-done(((f32[4,1,16384]{2,1,0:T(1,128)}), f32[4,1,16384]{2,1,0:T(1,128)S(1)}, u32[]{:S(2)}, u32[]{:S(2)}) %all-to-all-start) | async-done | bytes 262176 | tf_op jit(solution)/shard_map/all_to_all | solution.py:136
  82.7 1.3 %reduce.9 = f32[4,16384]{1,0:T(4,128)S(1)} reduce(f32[4,1,16384]{2,1,0:T(1,128)S(1)} %all-to-all-done, f32[]{:T(128)} %broadcast.118), dimensions={1}, to_apply=%all_to_all.6.reduce_sub_computation | reduce | bytes 524292 | tf_op jit(solution)/shard_map/all_to_all | solution.py:136
  84.4 1.3 %fusion.35 = bf16[2,4,1,32,64]{4,2,3,1,0:T(2,128)(2,1)S(1)} fusion(f32[4,2,4,1,1]{0,3,4,2,1:T(1,128)S(1)} %copy.173, f32[4,32,2,4,64]{4,3,2,1,0:T(4,128)S(1)} %bitcast.123), kind=kOutput, calls=%fused_computation.69 | convolution fusion | flops 786432 | bytes 295040 | tf_op jit(solution)/shard_map/kge,kngep->ngep/dot_general | solution.py:144
  85.7 1.3 %convolution_bitcast_fusion.3 = f32[4,32,2,4,64]{4,0,1,3,2:T(4,128)S(1)} fusion(f32[4,32,2,4,64]{4,3,2,1,0:T(4,128)S(1)} %bitcast.124, f32[4,2,4]{0,2,1:T(4,128)S(1)} %copy.156, f32[4,2,4]{0,2,1:T(4,128)S(1)} %copy.155, pred[4,4]{1,0:T(4,128)(4,1)S(1)} %copy-done.30), kind=kOutput, calls=%fused_computation.10 | convolution fusion | flops 3145984 | bytes 524560 | tf_op jit(solution)/shard_map/jkge,kngep->jngep/dot_general | solution.py:140
  87.1 1.0 reshape.276
  88.1 3.4 %all-to-all-start.1 = ((f32[4,1,16384]{2,1,0:T(1,128)}), f32[4,1,16384]{2,1,0:T(1,128)S(1)}, u32[]{:S(2)}, u32[]{:S(2)}) async-start(f32[4,1,16384]{2,1,0:T(1,128)} %reshape.276), calls=%async_computation.1 | async-start | bytes 524288 | tf_op jit(solution)/shard_map/all_to_all | solution.py:147
  91.9 12.2 %psum.31 = f32[2,4,64]{2,1,0:T(4,128)S(1)} all-reduce(f32[2,4,64]{2,1,0:T(4,128)S(1)} %bitcast.137), channel_id=1, replica_groups=mesh['grp'=2,'sp'=4,'tp'=4] {'sp'}, use_global_device_ids=true, to_apply=%region_8.9 | all-reduce | flops 512 | bytes 4096 | tf_op jit(solution)/shard_map/psum | solution.py:200
  104.5 0.7 convert_element_type.211
  105.3 0.8 multiply_convert_fusion.7
  106.9 1.3 %reduce.10 = f32[4,16384]{1,0:T(4,128)S(1)} reduce(f32[4,1,16384]{2,1,0:T(1,128)S(1)} %all-to-all-done.1, f32[]{:T(128)} %broadcast.118), dimensions={1}, to_apply=%all_to_all.8.reduce_sub_computation | reduce | bytes 524292 | tf_op jit(solution)/shard_map/all_to_all | solution.py:147
  108.5 0.9 copy.160
  109.4 2.3 %fusion.1 = f32[4,128,2,4,64]{1,4,3,2,0:T(8,128)S(1)} fusion(f32[4,128,2,4,64]{1,4,3,2,0:T(8,128)} %convolution_bitcast_fusion.2, f32[1,128,2,4,64]{1,4,3,2,0:T(8,128)} %get-tuple-element.41, f32[1,128,2,4,64]{1,4,3,2,0:T(8,128)} %get-tuple-element.42, f32[1,128,2,4,64]{1,4,3,2,0:T(8,128)} %get-tuple-element.43, f32[4]{0:T(128)S(1)} %copy-done.31, ...), kind=kOutput, calls=%fused_computation.4 | convolution fusion | flops 404488192 | bytes 3424400 | tf_op jit(solution)/shard_map/blgn,bngep->blgep/dot_general | solution.py:164
  111.7 1.8 %copy.184 = f32[4,128,2,4,64]{4,3,2,1,0:T(4,128)} copy(f32[4,128,2,4,64]{1,4,3,2,0:T(8,128)S(1)} %fusion.1) | data formatting | bytes 2097152 | tf_op jit(solution)/shard_map/reshape | solution.py:170
  113.5 3.5 %reshape.263 = f32[512,512]{1,0:T(8,128)} reshape(f32[4,128,2,4,64]{4,3,2,1,0:T(4,128)} %copy.184) | data formatting | bytes 2097152 | tf_op jit(solution)/shard_map/reshape | solution.py:170
  117.0 4.6 %fusion.93 = (f32[512,512]{1,0:T(8,128)}, f32[512,512]{1,0:T(8,128)}) fusion(bf16[512,2048]{1,0:T(8,128)(2,1)S(1)} %copy-done, bf16[2048,512]{1,0:T(8,128)(2,1)} %param.20, f32[512,512]{1,0:T(8,128)} %reshape.263, bf16[512,512]{1,0:T(8,128)(2,1)S(1)} %copy-done.2, f32[512]{0:T(512)S(1)} %copy-done.25), kind=kOutput, calls=%fused_computation.190 | convolution fusion | flops 1076625408 | bytes 7866368 | tf_op jit(solution)/shard_map/dot_general | solution.py:25
  121.7 1.9 %mul.516 = f32[512,2,256]{2,1,0:T(2,128)S(1)} reshape(f32[512,512]{1,0:T(8,128)} %get-tuple-element.63) | data formatting | bytes 2097152 | tf_op jit(solution)/shard_map/mul | solution.py:39
  125.4 1.1 multiply_convert_fusion.2
  (144 shorter events, 16.2 us)
Async XLA Ops:
  0.6 1.6 %copy-start = (bf16[512,2048]{1,0:T(8,128)(2,1)S(1)}, bf16[512,2048]{1,0:T(8,128)(2,1)}, u32[]{:S(2)}) copy-start(bf16[512,2048]{1,0:T(8,128)(2,1)} %param.15) | copy-start | bytes 6291460
  0.6 9.8 %copy-start.6 = (bf16[2048,256]{1,0:T(8,128)(2,1)S(1)}, bf16[2048,256]{1,0:T(8,128)(2,1)}, u32[]{:S(2)}) copy-start(bf16[2048,256]{1,0:T(8,128)(2,1)} %param.19) | copy-start | bytes 3145732
  4.2 11.3 %copy-start.3 = (bf16[2048,512]{1,0:T(8,128)(2,1)S(1)}, bf16[2048,512]{1,0:T(8,128)(2,1)}, u32[]{:S(2)}) copy-start(bf16[2048,512]{1,0:T(8,128)(2,1)} %param.17) | copy-start | bytes 6291460
  4.7 55.0 %collective-permute-start.2 = (bf16[3,256]{1,0:T(4,128)(2,1)}, bf16[3,256]{1,0:T(4,128)(2,1)}, u32[]{:S(2)}, u32[]{:S(2)}) collective-permute-start(bf16[3,256]{1,0:T(4,128)(2,1)} %get-tuple-element.57), channel_id=1, source_target_pairs={{0,4},{4,8},{8,12},{1,5},{5,9},{9,13},{2,6},{6,10},{10,14},{3,7},{... | collective-permute-start | bytes 4616 | tf_op jit(solution)/shard_map/ppermute | solution.py:16
  11.1 0.7 copy-start.10
  11.8 10.3 %copy-start.23 = (bf16[2048]{0:T(1024)(128)(2,1)S(1)}, bf16[2048]{0:T(1024)(128)(2,1)}, u32[]{:S(2)}) copy-start(bf16[2048]{0:T(1024)(128)(2,1)} %param.16) | copy-start | bytes 12292
  11.8 10.3 %copy-start.5 = (bf16[2048,256]{1,0:T(8,128)(2,1)S(1)}, bf16[2048,256]{1,0:T(8,128)(2,1)}, u32[]{:S(2)}) copy-start(bf16[2048,256]{1,0:T(8,128)(2,1)} %param.18) | copy-start | bytes 3145732
  11.8 49.6 %collective-permute-start.1 = (bf16[3,256]{1,0:T(4,128)(2,1)}, bf16[3,256]{1,0:T(4,128)(2,1)}, u32[]{:S(2)}, u32[]{:S(2)}) collective-permute-start(bf16[3,256]{1,0:T(4,128)(2,1)} %get-tuple-element.54), channel_id=1, source_target_pairs={{0,4},{4,8},{8,12},{1,5},{5,9},{9,13},{2,6},{6,10},{10,14},{3,7},{... | collective-permute-start | bytes 4616 | tf_op jit(solution)/shard_map/ppermute | solution.py:16
  16.7 0.8 copy-start.8
  18.1 44.7 %collective-permute-start = (bf16[3,512]{1,0:T(4,128)(2,1)}, bf16[3,512]{1,0:T(4,128)(2,1)}, u32[]{:S(2)}, u32[]{:S(2)}) collective-permute-start(bf16[3,512]{1,0:T(4,128)(2,1)} %get-tuple-element.52), channel_id=1, source_target_pairs={{0,4},{4,8},{8,12},{1,5},{5,9},{9,13},{2,6},{6,10},{10,14},{3,7},{... | collective-permute-start | bytes 9224 | tf_op jit(solution)/shard_map/ppermute | solution.py:16
  21.6 2.3 %copy-start.4 = (bf16[2048,512]{1,0:T(8,128)(2,1)S(1)}, bf16[2048,512]{1,0:T(8,128)(2,1)}, u32[]{:S(2)}) copy-start(bf16[2048,512]{1,0:T(8,128)(2,1)} %param.17) | copy-start | bytes 6291460
  22.1 2.2 %copy-start.33 = (f32[32]{0:T(128)S(1)}, f32[32]{0:T(128)}, u32[]{:S(2)}) copy-start(f32[32]{0:T(128)} %param.26) | copy-start | bytes 388
  22.2 2.3 %copy-start.32 = (f32[32]{0:T(128)S(1)}, f32[32]{0:T(128)}, u32[]{:S(2)}) copy-start(f32[32]{0:T(128)} %param.25) | copy-start | bytes 388
  22.2 3.0 %copy-start.12 = (f32[512,8]{0,1:T(8,128)S(1)}, f32[512,8]{0,1:T(8,128)}, u32[]{:S(2)}) copy-start(f32[512,8]{0,1:T(8,128)} %param.27) | copy-start | bytes 49156
  22.4 2.0 %copy-start.13 = (bf16[2048,32]{0,1:T(8,128)(2,1)S(1)}, bf16[2048,32]{0,1:T(8,128)(2,1)}, u32[]{:S(2)}) copy-start(bf16[2048,32]{0,1:T(8,128)(2,1)} %param.21) | copy-start | bytes 393220
  25.8 21.5 %copy-start.26 = (bf16[4,1024]{1,0:T(4,128)(2,1)S(1)}, bf16[4,1024]{1,0:T(4,128)(2,1)}, u32[]{:S(2)}) copy-start(bf16[4,1024]{1,0:T(4,128)(2,1)} %param.23) | copy-start | bytes 24580
  26.1 23.0 %copy-start.27 = (bf16[4,1024]{1,0:T(4,128)(2,1)S(1)}, bf16[4,1024]{1,0:T(4,128)(2,1)}, u32[]{:S(2)}) copy-start(bf16[4,1024]{1,0:T(4,128)(2,1)} %param.24) | copy-start | bytes 24580
  27.1 25.3 %copy-start.22 = (bf16[4,2048]{1,0:T(4,128)(2,1)S(1)}, bf16[4,2048]{1,0:T(4,128)(2,1)}, u32[]{:S(2)}) copy-start(bf16[4,2048]{1,0:T(4,128)(2,1)} %param.22) | copy-start | bytes 49156
  57.6 3.9 %copy-start.11 = (bf16[512,256]{1,0:T(8,128)(2,1)S(1)}, bf16[512,256]{1,0:T(8,128)(2,1)}, u32[]{:S(2)}) copy-start(bf16[512,256]{1,0:T(8,128)(2,1)} %copy-done.10) | copy-start | bytes 786436
  59.1 3.1 %copy-start.18 = (f32[1,256]{1,0:T(1,128)S(1)}, f32[1,256]{1,0:T(1,128)}, u32[]{:S(2)}) copy-start(f32[1,256]{1,0:T(1,128)} %get-tuple-element.24) | copy-start | bytes 3076
  59.1 3.2 %copy-start.19 = (f32[1,256]{1,0:T(1,128)S(1)}, f32[1,256]{1,0:T(1,128)}, u32[]{:S(2)}) copy-start(f32[1,256]{1,0:T(1,128)} %get-tuple-element.25) | copy-start | bytes 3076
  59.1 3.2 %copy-start.20 = (f32[1,256]{1,0:T(1,128)S(1)}, f32[1,256]{1,0:T(1,128)}, u32[]{:S(2)}) copy-start(f32[1,256]{1,0:T(1,128)} %get-tuple-element.26) | copy-start | bytes 3076
  59.1 3.2 %copy-start.21 = (f32[1,256]{1,0:T(1,128)S(1)}, f32[1,256]{1,0:T(1,128)}, u32[]{:S(2)}) copy-start(f32[1,256]{1,0:T(1,128)} %get-tuple-element.27) | copy-start | bytes 3076
  61.5 1.3 %copy-start.9 = (bf16[512,512]{1,0:T(8,128)(2,1)S(1)}, bf16[512,512]{1,0:T(8,128)(2,1)}, u32[]{:S(2)}) copy-start(bf16[512,512]{1,0:T(8,128)(2,1)} %copy-done.8) | copy-start | bytes 1572868
  65.0 4.5 %copy-start.1 = (bf16[512,512]{1,0:T(8,128)(2,1)}, bf16[512,512]{1,0:T(8,128)(2,1)S(1)}, u32[]{:S(2)}) copy-start(bf16[512,512]{1,0:T(8,128)(2,1)S(1)} %multiply_convert_fusion.4) | copy-start | bytes 1572868
  66.0 3.5 %copy-start.14 = (f32[2,4]{1,0:T(2,128)S(1)}, f32[2,4]{1,0:T(2,128)}, u32[]{:S(2)}) copy-start(f32[2,4]{1,0:T(2,128)} %get-tuple-element.48) | copy-start | bytes 100
  66.0 3.5 %copy-start.15 = (f32[2,4]{1,0:T(2,128)S(1)}, f32[2,4]{1,0:T(2,128)}, u32[]{:S(2)}) copy-start(f32[2,4]{1,0:T(2,128)} %get-tuple-element.49) | copy-start | bytes 100
  68.0 1.6 %copy-start.16 = (f32[2,4]{1,0:T(2,128)S(1)}, f32[2,4]{1,0:T(2,128)}, u32[]{:S(2)}) copy-start(f32[2,4]{1,0:T(2,128)} %get-tuple-element.50) | copy-start | bytes 100
  68.0 1.6 %copy-start.17 = (f32[2,4]{1,0:T(2,128)S(1)}, f32[2,4]{1,0:T(2,128)}, u32[]{:S(2)}) copy-start(f32[2,4]{1,0:T(2,128)} %get-tuple-element.51) | copy-start | bytes 100
  72.0 10.2 %all-to-all-start = ((f32[4,1,16384]{2,1,0:T(1,128)}), f32[4,1,16384]{2,1,0:T(1,128)S(1)}, u32[]{:S(2)}, u32[]{:S(2)}) async-start(f32[4,1,16384]{2,1,0:T(1,128)} %reshape.274), calls=%async_computation | async-start | bytes 524288 | tf_op jit(solution)/shard_map/all_to_all | solution.py:136
  75.9 9.8 %copy-start.30 = (pred[4,4]{1,0:T(4,128)(4,1)S(1)}, pred[4,4]{1,0:T(4,128)(4,1)}, u32[]{:S(2)}) copy-start(pred[4,4]{1,0:T(4,128)(4,1)} %iota_compare_fusion.1) | copy-start | bytes 52
  84.3 7.2 %copy-start.28 = (f32[2,4]{1,0:T(2,128)S(1)}, f32[2,4]{1,0:T(2,128)}, u32[]{:S(2)}) copy-start(f32[2,4]{1,0:T(2,128)} %mul.529) | copy-start | bytes 100
  84.3 7.4 %copy-start.24 = (bf16[2,32,1,1]{1,0,2,3:T(2,128)(2,1)S(1)}, bf16[2,32,1,1]{1,0,2,3:T(2,128)(2,1)}, u32[]{:S(2)}) copy-start(bf16[2,32,1,1]{1,0,2,3:T(2,128)(2,1)} %fusion.81) | copy-start | bytes 388
  85.7 18.4 %copy-start.29 = (f32[2,4]{1,0:T(2,128)S(1)}, f32[2,4]{1,0:T(2,128)}, u32[]{:S(2)}) copy-start(f32[2,4]{1,0:T(2,128)} %mul.552) | copy-start | bytes 100
  88.1 18.8 %all-to-all-start.1 = ((f32[4,1,16384]{2,1,0:T(1,128)}), f32[4,1,16384]{2,1,0:T(1,128)S(1)}, u32[]{:S(2)}, u32[]{:S(2)}) async-start(f32[4,1,16384]{2,1,0:T(1,128)} %reshape.276), calls=%async_computation.1 | async-start | bytes 524288 | tf_op jit(solution)/shard_map/all_to_all | solution.py:147
  91.5 17.9 %copy-start.31 = (f32[4]{0:T(128)S(1)}, f32[4]{0:T(128)}, u32[]{:S(2)}) copy-start(f32[4]{0:T(128)} %pad.6.clone) | copy-start | bytes 52
  113.5 3.5 %copy-start.2 = (bf16[512,512]{1,0:T(8,128)(2,1)S(1)}, bf16[512,512]{1,0:T(8,128)(2,1)}, u32[]{:S(2)}) copy-start(bf16[512,512]{1,0:T(8,128)(2,1)} %copy-done.1) | copy-start | bytes 1572868
  113.5 3.5 %copy-start.25 = (f32[512]{0:T(512)S(1)}, f32[512]{0:T(512)}, u32[]{:S(2)}) copy-start(f32[512]{0:T(512)} %mul.510) | copy-start | bytes 6148
  124.2 1.2 copy-start.7
where the time goes:
time: 127 us; the launch traced here: 126 us
  blocking collectives  30.3 us (24%)
  local copies, waits for them, and re-layouts  28.8 us (23%)
  matrix products  22.6 us (18%)
  other arithmetic  20.4 us (16%)
  starting transfers between devices  19.8 us (16%)
  waiting for transfers between devices  3.3 us (3%)
    ppermute x3, starting transfers between devices, passed_along(): return lax.ppermute(block, axis, route)  12.8 us
    dot_general x8, matrix products, project(): jnp.dot(operand, weights, preferred_element_type=jnp.float32)  12.6 us
    psum x1, blocking collectives, on_device(): reading = lax.psum(partial_value, 'sp')  12.2 us
    psum x1, blocking collectives, from_root(): return lax.psum(kept, axis)  10.5 us
    all_gather x1, blocking collectives, on_device(): lax.all_gather(shard_fading_factor[None], 'sp', axis=0, tiled=True)  7.58 us
    unnamed x75, local copies, waits for them, and re-layouts  6.63 us
    reshape x2, local copies, waits for them, and re-layouts, on_device(): (inner_part + carried_part).reshape(row_count, head_count, HEAD)  5.28 us
    all_to_all x1, starting transfers between devices, on_device(): lax.all_to_all(running[None], 'sp', split_axis=1, concat_axis=0, tiled=True)  3.58 us
  transfers between devices with their start and end apart: 5, of which 1 were waited for; matrix products, arithmetic and copies ran while one was open for 26% of the time, Pallas kernels for 0%

commit v1 on v0

--- a/solution.py
+++ b/solution.py
@@ -18,7 +18,7 @@
 
 def from_root(value, axis, source):
     kept = jnp.where(lax.axis_index(axis) == source, value, 0).astype(value.dtype)
-    return lax.psum(kept, axis)
+    return jnp.sum(lax.all_gather(kept, axis), axis=0)
 
 
 def project(operand, weights):

time: 127 us -> 152 us (1.20)
  blocking collectives: 30.3 us -> 56.9 us
    all_gather x0 -> x3, blocking collectives: none -> 37.1 us  [from_root(): return jnp.sum(lax.all_gather(kept, axis), axis=0)]
    psum x1 -> x0, blocking collectives: 10.5 us -> none  [from_root(): return lax.psum(kept, axis)]
    unnamed x0 -> x3, other arithmetic: none -> 1.75 us
    unnamed x75 -> x77, local copies, waits for them, and re-layouts: 6.63 us -> 6.58 us
  transfers between devices with their start and end apart: 5 -> 5, of which waited for: 1 -> 1; matrix products, arithmetic and copies ran while one was open for 26% -> 20% of each run, Pallas kernels for 0% -> 0%
where the time goes in v1:
time: 152 us; the launch traced here: 151 us
  blocking collectives  56.9 us (37%)
  local copies, waits for them, and re-layouts  27.5 us (18%)
  matrix products  22.1 us (15%)
  other arithmetic  20.4 us (13%)
  starting transfers between devices  19.8 us (13%)
  waiting for transfers between devices  3.31 us (2%)
    all_gather x3, blocking collectives, from_root(): return jnp.sum(lax.all_gather(kept, axis), axis=0)  37.1 us
    ppermute x3, starting transfers between devices, passed_along(): return lax.ppermute(block, axis, route)  12.8 us
    dot_general x8, matrix products, project(): jnp.dot(operand, weights, preferred_element_type=jnp.float32)  12.6 us
    psum x1, blocking collectives, on_device(): reading = lax.psum(partial_value, 'sp')  12.2 us
    all_gather x1, blocking collectives, on_device(): lax.all_gather(shard_fading_factor[None], 'sp', axis=0, tiled=True)  7.58 us
    unnamed x77, local copies, waits for them, and re-layouts  6.58 us
    reshape x2, local copies, waits for them, and re-layouts, on_device(): (inner_part + carried_part).reshape(row_count, head_count, HEAD)  5.32 us
    all_to_all x1, starting transfers between devices, on_device(): lax.all_to_all(running[None], 'sp', split_axis=1, concat_axis=0, tiled=True)  3.58 us
  transfers between devices with their start and end apart: 5, of which 1 were waited for; matrix products, arithmetic and copies ran while one was open for 20% of the time, Pallas kernels for 0%

profile of v1, /device:TPU:0, one launch (start us, length us, event | category | flops | bytes accessed | tf_op | source)
XLA Modules:
  0.0 151.2 jit_solution(16889777510640651780)
XLA Ops:
  0.7 1.6 %copy-done = bf16[512,2048]{1,0:T(8,128)(2,1)S(1)} copy-done((bf16[512,2048]{1,0:T(8,128)(2,1)S(1)}, bf16[512,2048]{1,0:T(8,128)(2,1)}, u32[]{:S(2)}) %copy-start) | copy-done | bytes 2097176
  2.2 1.9 %convolution_convert_fusion.2 = bf16[512,256]{1,0:T(8,128)(2,1)S(1)} fusion(bf16[512,2048]{1,0:T(8,128)(2,1)S(1)} %copy-done, bf16[2048,256]{1,0:T(8,128)(2,1)} %param.18), kind=kOutput, calls=%fused_computation.11 | convolution fusion | flops 537001984 | bytes 3407872 | tf_op jit(solution)/shard_map/dot_general | solution.py:25
  4.8 5.7 %collective-permute-start.2 = (bf16[3,256]{1,0:T(4,128)(2,1)}, bf16[3,256]{1,0:T(4,128)(2,1)}, u32[]{:S(2)}, u32[]{:S(2)}) collective-permute-start(bf16[3,256]{1,0:T(4,128)(2,1)} %get-tuple-element.54), channel_id=1, source_target_pairs={{0,4},{4,8},{8,12},{1,5},{5,9},{9,13},{2,6},{6,10},{10,14},{3,7},{... | collective-permute-start | bytes 4616 | tf_op jit(solution)/shard_map/ppermute | solution.py:16
  10.4 0.7 convolution_convert_fusion.3
  11.7 3.6 %collective-permute-start.1 = (bf16[3,256]{1,0:T(4,128)(2,1)}, bf16[3,256]{1,0:T(4,128)(2,1)}, u32[]{:S(2)}, u32[]{:S(2)}) collective-permute-start(bf16[3,256]{1,0:T(4,128)(2,1)} %get-tuple-element.52), channel_id=1, source_target_pairs={{0,4},{4,8},{8,12},{1,5},{5,9},{9,13},{2,6},{6,10},{10,14},{3,7},{... | collective-permute-start | bytes 4616 | tf_op jit(solution)/shard_map/ppermute | solution.py:16
  15.3 1.3 convolution_convert_fusion.1
  16.6 0.8 copy-done.8
  18.0 3.5 %collective-permute-start = (bf16[3,512]{1,0:T(4,128)(2,1)}, bf16[3,512]{1,0:T(4,128)(2,1)}, u32[]{:S(2)}, u32[]{:S(2)}) collective-permute-start(bf16[3,512]{1,0:T(4,128)(2,1)} %get-tuple-element.50), channel_id=1, source_target_pairs={{0,4},{4,8},{8,12},{1,5},{5,9},{9,13},{2,6},{6,10},{10,14},{3,7},{... | collective-permute-start | bytes 9224 | tf_op jit(solution)/shard_map/ppermute | solution.py:16
  22.3 1.5 fusion.94
  26.5 2.0 %fusion.97 = f32[1,512]{1,0:T(1,128)S(1)} fusion(bf16[2048,1]{0,1:T(2,128)(2,1)S(1)} %reshape.263, bf16[2048,512]{1,0:T(8,128)(2,1)} %param.20), kind=kOutput, calls=%fused_computation.195 | convolution fusion | flops 2097152 | bytes 2103296 | tf_op jit(solution)/shard_map/dot_general | solution.py:25
  28.5 11.9 %all-gather.6 = bf16[4,3,256]{2,1,0:T(4,128)(2,1)S(1)} all-gather(bf16[1,3,256]{2,1,0:T(4,128)(2,1)S(1)} %get-tuple-element.53), channel_id=4, replica_groups=mesh['grp'=2,'sp'=4,'tp'=4] {'sp'}, dimensions={0}, use_global_device_ids=true | all-gather | bytes 7680 | tf_op jit(solution)/shard_map/all_gather | solution.py:21
  40.5 0.7 convert_convert_fusion
  41.3 11.9 %all-gather.5 = bf16[4,3,256]{2,1,0:T(4,128)(2,1)S(1)} all-gather(bf16[1,3,256]{2,1,0:T(4,128)(2,1)S(1)} %get-tuple-element.51), channel_id=3, replica_groups=mesh['grp'=2,'sp'=4,'tp'=4] {'sp'}, dimensions={0}, use_global_device_ids=true | all-gather | bytes 7680 | tf_op jit(solution)/shard_map/all_gather | solution.py:21
  53.3 7.6 %all-gather.4 = f32[4,2,4]{2,1,0:T(2,128)S(1)} all-gather(f32[1,2,4]{2,1,0:T(2,128)S(1)} %bitcast.158), channel_id=2, replica_groups=mesh['grp'=2,'sp'=4,'tp'=4] {'sp'}, dimensions={0}, use_global_device_ids=true | all-gather | bytes 160 | tf_op jit(solution)/shard_map/all_gather | solution.py:132
  60.9 13.2 %all-gather.7 = bf16[4,3,512]{2,1,0:T(4,128)(2,1)S(1)} all-gather(bf16[1,3,512]{2,1,0:T(4,128)(2,1)S(1)} %get-tuple-element.49), channel_id=5, replica_groups=mesh['grp'=2,'sp'=4,'tp'=4] {'sp'}, dimensions={0}, use_global_device_ids=true | all-gather | bytes 15360 | tf_op jit(solution)/shard_map/all_gather | solution.py:21
  74.1 1.0 copy.149
  75.3 0.7 convert_reduce_fusion.1
  75.9 2.4 %fusion.90 = (f32[4,128,2,4]{3,2,1,0:T(2,128)}, f32[4,128,2,4]{3,2,1,0:T(2,128)S(1)}) fusion(f32[4,128,2,4]{3,2,1,0:T(2,128)S(1)} %fusion.92, f32[4,128,2,4]{3,2,1,0:T(2,128)} %copy.149, f32[4,2,4]{2,1,0:T(2,128)S(1)} %get-tuple-element.44), kind=kLoop, calls=%fused_computation.187 | loop fusion | flops 8192 | bytes 65664 | tf_op jit(solution)/shard_map/exp | solution.py:164
  82.3 1.3 copy.148
  84.4 0.7 maximum_convert_fusion.1
  85.1 1.0 multiply_convert_fusion.6
  86.2 0.8 maximum_convert_fusion.2
  87.5 0.8 maximum_convert_fusion
  88.3 1.3 multiply_convert_fusion.4
  89.7 1.0 copy.140
  90.7 2.0 %reshape.229 = bf16[4,128,2,4,64]{1,0,4,3,2:T(4,128)(2,1)} reshape(bf16[512,512]{0,1:T(8,128)(2,1)} %copy.140) | data formatting | bytes 1048576 | tf_op jit(solution)/shard_map/reshape | solution.py:109
  92.7 1.3 multiply_convert_fusion.3
  94.3 1.0 slice_add_fusion
  95.5 1.2 reshape.286
  96.7 3.6 %all-to-all-start = ((f32[4,1,16384]{2,1,0:T(1,128)}), f32[4,1,16384]{2,1,0:T(1,128)S(1)}, u32[]{:S(2)}, u32[]{:S(2)}) async-start(f32[4,1,16384]{2,1,0:T(1,128)} %reshape.286), calls=%async_computation | async-start | bytes 524288 | tf_op jit(solution)/shard_map/all_to_all | solution.py:136
  100.6 2.9 %convolution_bitcast_fusion.2 = f32[4,128,2,4,64]{1,4,3,2,0:T(8,128)} fusion(f32[4,2,4,128]{3,2,1,0:T(4,128)S(1)} %copy.146, f32[4,2,4,128]{3,2,1,0:T(4,128)S(1)} %copy.144, f32[4,2,128,128]{3,2,1,0:T(8,128)S(1)} %fusion.40, pred[128,128]{1,0:T(8,128)(4,1)S(1)} %iota_compare_fusion, bf16[4,128,2,4,64]{1,0,4,3,2:T(4,128)(2,1)} %reshape.229), kind=kOutput, calls=%fused_computation.5 | convolution fusion | flops 69730304 | bytes 2146304 | tf_op jit(solution)/shard_map/bgels,bsgep->blgep/dot_general | solution.py:160
  103.6 3.3 %all-to-all-done = f32[4,1,16384]{2,1,0:T(1,128)S(1)} async-done(((f32[4,1,16384]{2,1,0:T(1,128)}), f32[4,1,16384]{2,1,0:T(1,128)S(1)}, u32[]{:S(2)}, u32[]{:S(2)}) %all-to-all-start) | async-done | bytes 262176 | tf_op jit(solution)/shard_map/all_to_all | solution.py:136
  107.4 1.3 reduce.15
  109.1 1.3 fusion.35
  110.4 1.3 convolution_bitcast_fusion.3
  111.8 1.0 reshape.288
  112.8 3.4 %all-to-all-start.1 = ((f32[4,1,16384]{2,1,0:T(1,128)}), f32[4,1,16384]{2,1,0:T(1,128)S(1)}, u32[]{:S(2)}, u32[]{:S(2)}) async-start(f32[4,1,16384]{2,1,0:T(1,128)} %reshape.288), calls=%async_computation.1 | async-start | bytes 524288 | tf_op jit(solution)/shard_map/all_to_all | solution.py:147
  116.6 12.2 %psum.7 = f32[2,4,64]{2,1,0:T(4,128)S(1)} all-reduce(f32[2,4,64]{2,1,0:T(4,128)S(1)} %bitcast.143), channel_id=1, replica_groups=mesh['grp'=2,'sp'=4,'tp'=4] {'sp'}, use_global_device_ids=true, to_apply=%region_8.9 | all-reduce | flops 512 | bytes 4096 | tf_op jit(solution)/shard_map/psum | solution.py:200
  129.2 0.7 convert_element_type.217
  130.0 0.8 multiply_convert_fusion.7
  131.6 1.3 reduce.16
  133.2 0.9 copy.160
  134.1 2.3 %fusion.1 = f32[4,128,2,4,64]{1,4,3,2,0:T(8,128)S(1)} fusion(f32[4,128,2,4,64]{1,4,3,2,0:T(8,128)} %convolution_bitcast_fusion.2, f32[1,128,2,4,64]{1,4,3,2,0:T(8,128)} %get-tuple-element.38, f32[1,128,2,4,64]{1,4,3,2,0:T(8,128)} %get-tuple-element.39, f32[1,128,2,4,64]{1,4,3,2,0:T(8,128)} %get-tuple-element.40, f32[4]{0:T(128)S(1)} %copy-done.31, ...), kind=kOutput, calls=%fused_computation.4 | convolution fusion | flops 404488192 | bytes 3424400 | tf_op jit(solution)/shard_map/blgn,bngep->blgep/dot_general | solution.py:164
  136.5 1.8 %copy.184 = f32[4,128,2,4,64]{4,3,2,1,0:T(4,128)} copy(f32[4,128,2,4,64]{1,4,3,2,0:T(8,128)S(1)} %fusion.1) | data formatting | bytes 2097152 | tf_op jit(solution)/shard_map/reshape | solution.py:170
  138.2 3.5 %reshape.275 = f32[512,512]{1,0:T(8,128)} reshape(f32[4,128,2,4,64]{4,3,2,1,0:T(4,128)} %copy.184) | data formatting | bytes 2097152 | tf_op jit(solution)/shard_map/reshape | solution.py:170
  141.8 4.6 %fusion.91 = (f32[512,512]{1,0:T(8,128)}, f32[512,512]{1,0:T(8,128)}) fusion(bf16[512,2048]{1,0:T(8,128)(2,1)S(1)} %copy-done, bf16[2048,512]{1,0:T(8,128)(2,1)} %param.20, f32[512,512]{1,0:T(8,128)} %reshape.275, bf16[512,512]{1,0:T(8,128)(2,1)S(1)} %copy-done.2, f32[512]{0:T(512)S(1)} %copy-done.25), kind=kOutput, calls=%fused_computation.188 | convolution fusion | flops 1076625408 | bytes 7866368 | tf_op jit(solution)/shard_map/dot_general | solution.py:25
  146.4 1.9 %mul.516 = f32[512,2,256]{2,1,0:T(2,128)S(1)} reshape(f32[512,512]{1,0:T(8,128)} %get-tuple-element.60) | data formatting | bytes 2097152 | tf_op jit(solution)/shard_map/mul | solution.py:39
  150.1 1.1 multiply_convert_fusion.2
  (152 shorter events, 16.3 us)
Async XLA Ops:
  0.6 1.6 %copy-start = (bf16[512,2048]{1,0:T(8,128)(2,1)S(1)}, bf16[512,2048]{1,0:T(8,128)(2,1)}, u32[]{:S(2)}) copy-start(bf16[512,2048]{1,0:T(8,128)(2,1)} %param.15) | copy-start | bytes 6291460
  0.6 9.8 %copy-start.6 = (bf16[2048,256]{1,0:T(8,128)(2,1)S(1)}, bf16[2048,256]{1,0:T(8,128)(2,1)}, u32[]{:S(2)}) copy-start(bf16[2048,256]{1,0:T(8,128)(2,1)} %param.19) | copy-start | bytes 3145732
  4.2 7.6 %copy-start.10 = (bf16[512,256]{1,0:T(8,128)(2,1)}, bf16[512,256]{1,0:T(8,128)(2,1)S(1)}, u32[]{:S(2)}) copy-start(bf16[512,256]{1,0:T(8,128)(2,1)S(1)} %convolution_convert_fusion.2) | copy-start | bytes 786436
  4.2 11.2 %copy-start.3 = (bf16[2048,512]{1,0:T(8,128)(2,1)S(1)}, bf16[2048,512]{1,0:T(8,128)(2,1)}, u32[]{:S(2)}) copy-start(bf16[2048,512]{1,0:T(8,128)(2,1)} %param.17) | copy-start | bytes 6291460
  4.8 81.4 %collective-permute-start.2 = (bf16[3,256]{1,0:T(4,128)(2,1)}, bf16[3,256]{1,0:T(4,128)(2,1)}, u32[]{:S(2)}, u32[]{:S(2)}) collective-permute-start(bf16[3,256]{1,0:T(4,128)(2,1)} %get-tuple-element.54), channel_id=1, source_target_pairs={{0,4},{4,8},{8,12},{1,5},{5,9},{9,13},{2,6},{6,10},{10,14},{3,7},{... | collective-permute-start | bytes 4616 | tf_op jit(solution)/shard_map/ppermute | solution.py:16
  11.7 10.3 %copy-start.23 = (bf16[2048]{0:T(1024)(128)(2,1)S(1)}, bf16[2048]{0:T(1024)(128)(2,1)}, u32[]{:S(2)}) copy-start(bf16[2048]{0:T(1024)(128)(2,1)} %param.16) | copy-start | bytes 12292
  11.7 10.3 %copy-start.5 = (bf16[2048,256]{1,0:T(8,128)(2,1)S(1)}, bf16[2048,256]{1,0:T(8,128)(2,1)}, u32[]{:S(2)}) copy-start(bf16[2048,256]{1,0:T(8,128)(2,1)} %param.18) | copy-start | bytes 3145732
  11.7 72.7 %collective-permute-start.1 = (bf16[3,256]{1,0:T(4,128)(2,1)}, bf16[3,256]{1,0:T(4,128)(2,1)}, u32[]{:S(2)}, u32[]{:S(2)}) collective-permute-start(bf16[3,256]{1,0:T(4,128)(2,1)} %get-tuple-element.52), channel_id=1, source_target_pairs={{0,4},{4,8},{8,12},{1,5},{5,9},{9,13},{2,6},{6,10},{10,14},{3,7},{... | collective-permute-start | bytes 4616 | tf_op jit(solution)/shard_map/ppermute | solution.py:16
  16.6 0.8 copy-start.8
  18.0 69.5 %collective-permute-start = (bf16[3,512]{1,0:T(4,128)(2,1)}, bf16[3,512]{1,0:T(4,128)(2,1)}, u32[]{:S(2)}, u32[]{:S(2)}) collective-permute-start(bf16[3,512]{1,0:T(4,128)(2,1)} %get-tuple-element.50), channel_id=1, source_target_pairs={{0,4},{4,8},{8,12},{1,5},{5,9},{9,13},{2,6},{6,10},{10,14},{3,7},{... | collective-permute-start | bytes 9224 | tf_op jit(solution)/shard_map/ppermute | solution.py:16
  21.5 2.3 %copy-start.4 = (bf16[2048,512]{1,0:T(8,128)(2,1)S(1)}, bf16[2048,512]{1,0:T(8,128)(2,1)}, u32[]{:S(2)}) copy-start(bf16[2048,512]{1,0:T(8,128)(2,1)} %param.17) | copy-start | bytes 6291460
  22.0 2.2 %copy-start.33 = (f32[32]{0:T(128)S(1)}, f32[32]{0:T(128)}, u32[]{:S(2)}) copy-start(f32[32]{0:T(128)} %param.26) | copy-start | bytes 388
  22.1 2.3 %copy-start.32 = (f32[32]{0:T(128)S(1)}, f32[32]{0:T(128)}, u32[]{:S(2)}) copy-start(f32[32]{0:T(128)} %param.25) | copy-start | bytes 388
  22.1 2.4 %copy-start.12 = (f32[512,8]{0,1:T(8,128)S(1)}, f32[512,8]{0,1:T(8,128)}, u32[]{:S(2)}) copy-start(f32[512,8]{0,1:T(8,128)} %param.27) | copy-start | bytes 49156
  22.3 2.0 %copy-start.13 = (bf16[2048,32]{0,1:T(8,128)(2,1)S(1)}, bf16[2048,32]{0,1:T(8,128)(2,1)}, u32[]{:S(2)}) copy-start(bf16[2048,32]{0,1:T(8,128)(2,1)} %param.21) | copy-start | bytes 393220
  25.2 15.3 %copy-start.26 = (bf16[4,1024]{1,0:T(4,128)(2,1)S(1)}, bf16[4,1024]{1,0:T(4,128)(2,1)}, u32[]{:S(2)}) copy-start(bf16[4,1024]{1,0:T(4,128)(2,1)} %param.23) | copy-start | bytes 24580
  25.5 49.8 %copy-start.27 = (bf16[4,1024]{1,0:T(4,128)(2,1)S(1)}, bf16[4,1024]{1,0:T(4,128)(2,1)}, u32[]{:S(2)}) copy-start(bf16[4,1024]{1,0:T(4,128)(2,1)} %param.24) | copy-start | bytes 24580
  26.5 51.9 %copy-start.22 = (bf16[4,2048]{1,0:T(4,128)(2,1)S(1)}, bf16[4,2048]{1,0:T(4,128)(2,1)}, u32[]{:S(2)}) copy-start(bf16[4,2048]{1,0:T(4,128)(2,1)} %param.22) | copy-start | bytes 49156
  26.5 53.2 %copy-start.34 = (f32[32]{0:T(128)S(1)}, f32[32]{0:T(128)}, u32[]{:S(2)}) copy-start(f32[32]{0:T(128)} %param.28) | copy-start | bytes 388
  82.3 3.9 %copy-start.11 = (bf16[512,256]{1,0:T(8,128)(2,1)S(1)}, bf16[512,256]{1,0:T(8,128)(2,1)}, u32[]{:S(2)}) copy-start(bf16[512,256]{1,0:T(8,128)(2,1)} %copy-done.10) | copy-start | bytes 786436
  83.8 3.2 %copy-start.18 = (f32[1,256]{1,0:T(1,128)S(1)}, f32[1,256]{1,0:T(1,128)}, u32[]{:S(2)}) copy-start(f32[1,256]{1,0:T(1,128)} %get-tuple-element.28) | copy-start | bytes 3076
  83.8 3.2 %copy-start.19 = (f32[1,256]{1,0:T(1,128)S(1)}, f32[1,256]{1,0:T(1,128)}, u32[]{:S(2)}) copy-start(f32[1,256]{1,0:T(1,128)} %get-tuple-element.29) | copy-start | bytes 3076
  83.8 3.2 %copy-start.20 = (f32[1,256]{1,0:T(1,128)S(1)}, f32[1,256]{1,0:T(1,128)}, u32[]{:S(2)}) copy-start(f32[1,256]{1,0:T(1,128)} %get-tuple-element.30) | copy-start | bytes 3076
  83.8 3.2 %copy-start.21 = (f32[1,256]{1,0:T(1,128)S(1)}, f32[1,256]{1,0:T(1,128)}, u32[]{:S(2)}) copy-start(f32[1,256]{1,0:T(1,128)} %get-tuple-element.31) | copy-start | bytes 3076
  86.1 1.4 copy-start.9
  89.7 4.6 %copy-start.1 = (bf16[512,512]{1,0:T(8,128)(2,1)}, bf16[512,512]{1,0:T(8,128)(2,1)S(1)}, u32[]{:S(2)}) copy-start(bf16[512,512]{1,0:T(8,128)(2,1)S(1)} %multiply_convert_fusion.4) | copy-start | bytes 1572868
  90.7 3.6 %copy-start.14 = (f32[2,4]{1,0:T(2,128)S(1)}, f32[2,4]{1,0:T(2,128)}, u32[]{:S(2)}) copy-start(f32[2,4]{1,0:T(2,128)} %get-tuple-element.45) | copy-start | bytes 100
  90.7 3.6 %copy-start.15 = (f32[2,4]{1,0:T(2,128)S(1)}, f32[2,4]{1,0:T(2,128)}, u32[]{:S(2)}) copy-start(f32[2,4]{1,0:T(2,128)} %get-tuple-element.46) | copy-start | bytes 100
  92.7 1.6 %copy-start.16 = (f32[2,4]{1,0:T(2,128)S(1)}, f32[2,4]{1,0:T(2,128)}, u32[]{:S(2)}) copy-start(f32[2,4]{1,0:T(2,128)} %get-tuple-element.47) | copy-start | bytes 100
  92.7 1.6 %copy-start.17 = (f32[2,4]{1,0:T(2,128)S(1)}, f32[2,4]{1,0:T(2,128)}, u32[]{:S(2)}) copy-start(f32[2,4]{1,0:T(2,128)} %get-tuple-element.48) | copy-start | bytes 100
  96.7 10.2 %all-to-all-start = ((f32[4,1,16384]{2,1,0:T(1,128)}), f32[4,1,16384]{2,1,0:T(1,128)S(1)}, u32[]{:S(2)}, u32[]{:S(2)}) async-start(f32[4,1,16384]{2,1,0:T(1,128)} %reshape.286), calls=%async_computation | async-start | bytes 524288 | tf_op jit(solution)/shard_map/all_to_all | solution.py:136
  100.6 9.8 %copy-start.30 = (pred[4,4]{1,0:T(4,128)(4,1)S(1)}, pred[4,4]{1,0:T(4,128)(4,1)}, u32[]{:S(2)}) copy-start(pred[4,4]{1,0:T(4,128)(4,1)} %iota_compare_fusion.1) | copy-start | bytes 52
  109.0 7.2 %copy-start.28 = (f32[2,4]{1,0:T(2,128)S(1)}, f32[2,4]{1,0:T(2,128)}, u32[]{:S(2)}) copy-start(f32[2,4]{1,0:T(2,128)} %mul.529) | copy-start | bytes 100
  109.0 7.4 %copy-start.24 = (bf16[2,32,1,1]{1,0,2,3:T(2,128)(2,1)S(1)}, bf16[2,32,1,1]{1,0,2,3:T(2,128)(2,1)}, u32[]{:S(2)}) copy-start(bf16[2,32,1,1]{1,0,2,3:T(2,128)(2,1)} %fusion.81) | copy-start | bytes 388
  110.4 18.4 %copy-start.29 = (f32[2,4]{1,0:T(2,128)S(1)}, f32[2,4]{1,0:T(2,128)}, u32[]{:S(2)}) copy-start(f32[2,4]{1,0:T(2,128)} %mul.552) | copy-start | bytes 100
  112.8 18.8 %all-to-all-start.1 = ((f32[4,1,16384]{2,1,0:T(1,128)}), f32[4,1,16384]{2,1,0:T(1,128)S(1)}, u32[]{:S(2)}, u32[]{:S(2)}) async-start(f32[4,1,16384]{2,1,0:T(1,128)} %reshape.288), calls=%async_computation.1 | async-start | bytes 524288 | tf_op jit(solution)/shard_map/all_to_all | solution.py:147
  116.3 17.9 %copy-start.31 = (f32[4]{0:T(128)S(1)}, f32[4]{0:T(128)}, u32[]{:S(2)}) copy-start(f32[4]{0:T(128)} %pad.6.clone) | copy-start | bytes 52
  138.2 3.5 %copy-start.2 = (bf16[512,512]{1,0:T(8,128)(2,1)S(1)}, bf16[512,512]{1,0:T(8,128)(2,1)}, u32[]{:S(2)}) copy-start(bf16[512,512]{1,0:T(8,128)(2,1)} %copy-done.1) | copy-start | bytes 1572868
  138.2 3.5 %copy-start.25 = (f32[512]{0:T(512)S(1)}, f32[512]{0:T(512)}, u32[]{:S(2)}) copy-start(f32[512]{0:T(512)} %mul.510) | copy-start | bytes 6148
  148.9 1.2 copy-start.7
